TPU v7x, 32 devices: a whole 2x2x4 slice. The times are simulated.
32 devices in a mesh: ep: 16 (over z, x, core), tp: 2 (over y).
Axes of the slice: x: 2, y: 2, z: 4, core: 2. Of those that a mesh axis runs over, the one named last changes fastest.
Arguments:
- tokens: bfloat16 [192, 4096], P('ep', 'tp')
- norm_gain: float32 [4096], P('tp'), may hold values from 0.1 to 1.9
- routes: int32 [192, 6], P('ep'), may hold values from 0 to 15, all different within a row; in each aligned block of 12 rows (0 to 11, 12 to 23, ...) at most 5 rows name the same one
- route_weights: float32 [192, 6], P('ep'), may hold values from 0.05 to 1
- expert_gate: bfloat16 [16, 4096, 1024], P('ep', 'tp'), may hold values from -0.09375 to 0.09375
- expert_up: bfloat16 [16, 4096, 1024], P('ep', 'tp'), may hold values from -0.09375 to 0.09375
- expert_down: bfloat16 [16, 1024, 4096], P('ep', None, 'tp'), may hold values from -0.1875 to 0.1875
- shared_gate: bfloat16 [4096, 1024], P('tp'), may hold values from -0.09375 to 0.09375
- shared_up: bfloat16 [4096, 1024], P('tp'), may hold values from -0.09375 to 0.09375
- shared_down: bfloat16 [1024, 4096], P(None, 'tp'), may hold values from -0.1875 to 0.1875
Outputs:
- mixed: bfloat16 [192, 4096], P('ep', 'tp')
Inputs may be any that keep to these rules, and one draw needn't show every extreme that they name: `routes`: each row names 6 different experts; among the rows of one device no expert is named more than 5 times, and in some devices' rows one expert is named exactly 5 times.
All inputs are finite; a program needn't handle non-finite values.
Results may differ from a plain program's by a relative error of at most 0.0068.
Values may be sent and summed in bfloat16 or wider, within the bound.
No kernel may reach another device: no remote copies, remote signals or barrier semaphores. Data moves between devices by JAX's collectives and lax.ppermute only.
A program may use at most 64 MiB of HBM per device.

v0:
```python
import functools

import jax
import jax.numpy as jnp
from jax import lax
from jax.experimental import pallas as pl
from jax.experimental.pallas import tpu as pltpu
from jax.sharding import PartitionSpec as P


F32 = jnp.float32
BF16 = jnp.bfloat16
LANES = 128
N_HELD = 4
AHEAD = 10**12
VMEM = pl.BlockSpec(memory_space=pltpu.VMEM)
HBM = pl.BlockSpec(memory_space=pltpu.HBM)


def call(body, outs, ins, scratch=(), flops=0, limit=8):
    return pl.pallas_call(
        body,
        out_shape=outs,
        in_specs=list(ins),
        out_specs=jax.tree.map(lambda _: VMEM, outs),
        scratch_shapes=list(scratch),
        cost_estimate=pl.CostEstimate(flops=flops, bytes_accessed=0, transcendentals=0),
        compiler_params=pltpu.CompilerParams(vmem_limit_bytes=limit * 2**20),
    )


def stored(value):
    return pltpu.with_memory_space_constraint(value, pltpu.HBM)


def start_copies(pairs, sems):
    copies = [pltpu.make_async_copy(src, dst, sems.at[i]) for i, (src, dst) in enumerate(pairs)]
    for copy in copies:
        copy.start()
    return copies


def dot(a, b):
    return jnp.dot(a, b, preferred_element_type=F32)


def shard(size, index, chunk=0, chunks=1):
    part = size // chunks
    return pl.ds(pl.multiple_of(index * size + chunk * part, part), part)


def peer(step):
    return lax.rem(lax.axis_index("tp") + step, lax.axis_size("tp"))


def dispatch_body(cap, tok_hbm, routes_hbm, weight_hbm, out_ref, comb_ref, *scratch):
    wide, tok_ref, routes_ref, weight_ref, sems = scratch
    copies = start_copies(
        ((routes_hbm, routes_ref), (weight_hbm, weight_ref), (tok_hbm, tok_ref)), sems
    )
    tok, width = tok_ref.shape
    picks = routes_ref.shape[0]
    slots = comb_ref.shape[1]
    split = width // LANES
    slot = lax.broadcasted_iota(jnp.int32, (slots, tok), 0)
    expert = jnp.floor((slot.astype(F32) + 0.5) * (1.0 / cap)).astype(jnp.int32)
    rank = (slot - expert * cap).astype(F32)
    row = lax.broadcasted_iota(jnp.int32, (tok, tok), 0)
    col = lax.broadcasted_iota(jnp.int32, (tok, tok), 1)
    earlier = jnp.where(row < col, 1.0, 0.0).astype(BF16)
    copies[0].wait()
    copies[1].wait()
    routes = routes_ref[...]
    weights = weight_ref[...]
    scaled = 2.5 * weights / jnp.sum(weights, axis=0, keepdims=True)
    named = jnp.zeros((slots, tok), F32)
    gain = jnp.zeros((slots, tok), F32)
    for k in range(picks):
        same = routes[k : k + 1, :] == expert
        named = jnp.where(same, 1.0, named)
        gain = jnp.where(same, scaled[k : k + 1, :], gain)
    before = dot(named.astype(BF16), earlier)
    hit = jnp.where(before == rank, named, 0.0)
    pick = hit.astype(BF16)
    copies[2].wait()
    for q in range(0, split, 2):
        rows = dot(pick, tok_ref[:, q * LANES : (q + 2) * LANES])
        wide[pl.ds(q, slots, stride=split), :] = rows[:, :LANES]
        wide[pl.ds(q + 1, slots, stride=split), :] = rows[:, LANES:]
    out_ref[...] = wide[...].astype(BF16)
    comb_ref[...] = jnp.transpose(hit * gain)


def squares_tail(total):
    lane = lax.broadcasted_iota(jnp.int32, (total.shape[0], LANES), 1)
    high = total.astype(BF16).astype(F32)
    return jnp.where(lane == 0, high, jnp.where(lane == 1, total - high, 0.0))


def shared_in_body(tok_ref, gain_ref, gate_ref, up_ref, keep_ref, send_ref):
    hidden = gate_ref.shape[1]
    tok = tok_ref.shape[0]
    keep_ref[...] = jnp.zeros_like(keep_ref)
    values = tok_ref[...].astype(F32)
    keep_ref[:tok, 2 * hidden :] = squares_tail(jnp.sum(values * values, axis=1, keepdims=True))
    rows = (values * gain_ref[...]).astype(BF16)
    keep_ref[:tok, :hidden] = dot(rows, gate_ref[...])
    keep_ref[:tok, hidden : 2 * hidden] = dot(rows, up_ref[...])
    send_ref[...] = keep_ref[...].astype(BF16)


def row_scale(tail, width):
    return lax.rsqrt(jnp.sum(tail, axis=1, keepdims=True) / width + 1e-06)


def hidden_units(total, scale, hidden):
    gate = total[:, :hidden] * scale
    up = total[:, hidden : 2 * hidden] * scale
    return (gate / (1.0 + jnp.exp(-gate)) * up).astype(BF16)


def shared_out_body(width, keep_ref, *refs):
    recv_refs, down_ref, out_ref = refs[:-2], refs[-2], refs[-1]
    total = keep_ref[...]
    for recv in recv_refs:
        total = total + recv[...].astype(F32)
    hidden = down_ref.shape[0]
    act = hidden_units(total, row_scale(total[:, 2 * hidden :], width), hidden)
    out_ref[...] = dot(act, down_ref[...])[: out_ref.shape[0]]


def send_part(send, lhs_ref, gate_ref, up_ref, k, chunk, chunks):
    size = gate_ref.shape[1] // lax.axis_size("tp")
    part = size // chunks
    cols = shard(size, peer(k), chunk, chunks)
    send[:, :part] = dot(lhs_ref[...], gate_ref[:, cols]).astype(BF16)
    send[:, part : 2 * part] = dot(lhs_ref[...], up_ref[:, cols]).astype(BF16)


def expert_first_body(n_send, chunks, rows_ref, gain_ref, gate_ref, up_ref, *refs):
    refs = refs[N_HELD:]
    send_refs, (lhs_ref, tail_ref, wide) = refs[:n_send], refs[n_send:]
    slots, width = lhs_ref.shape
    split = width // LANES
    wide[...] = rows_ref[...].astype(F32)
    squares = jnp.zeros((slots, LANES), F32)
    for q in range(split):
        values = wide[pl.ds(q, slots, stride=split), :]
        squares = squares + values * values
        cols = slice(q * LANES, (q + 1) * LANES)
        lhs_ref[:, cols] = (values * gain_ref[:, cols]).astype(BF16)
    tail = squares_tail(jnp.sum(squares, axis=1, keepdims=True))
    tail_ref[...] = tail
    for k, send in enumerate(send_refs, 1):
        send_part(send, lhs_ref, gate_ref, up_ref, k, 0, chunks)
        send[:, -LANES:] = tail.astype(BF16)


def expert_later_body(chunk, chunks, lhs_ref, gate_ref, up_ref, *send_refs):
    for k, send in enumerate(send_refs, 1):
        send_part(send, lhs_ref, gate_ref, up_ref, k, chunk, chunks)


def expert_keep_body(lhs_ref, gate_ref, up_ref, *keep_refs):
    chunks = len(keep_refs)
    part = keep_refs[0].shape[1] // 2
    for chunk, keep in enumerate(keep_refs):
        cols = shard(part * chunks, peer(0), chunk, chunks)
        keep[:, :part] = dot(lhs_ref[...], gate_ref[:, cols])
        keep[:, part:] = dot(lhs_ref[...], up_ref[:, cols])


def first_mid_body(width, keep_ref, tail_ref, *refs):
    recv_refs, out_ref, scale_ref = refs[:-2], refs[-2], refs[-1]
    total, tail = keep_ref[...], tail_ref[...]
    part = out_ref.shape[1]
    for recv in recv_refs:
        total = total + recv[:, : 2 * part].astype(F32)
        tail = tail + recv[:, 2 * part :].astype(F32)
    scale = row_scale(tail, width)
    scale_ref[...] = jnp.broadcast_to(scale, scale_ref.shape)
    out_ref[...] = hidden_units(total, scale, part)


def later_mid_body(keep_ref, scale_ref, *refs):
    recv_refs, out_ref = refs[:-1], refs[-1]
    total = keep_ref[...]
    for recv in recv_refs:
        total = total + recv[...].astype(F32)
    out_ref[...] = hidden_units(total, scale_ref[:, :1], out_ref.shape[1])


def down_keep_body(down_ref, *refs):
    act_refs, acc_ref = refs[:-1], refs[-1]
    chunks = len(act_refs)
    size = act_refs[0].shape[1] * chunks
    act = jnp.concatenate([ref[...] for ref in act_refs], axis=1)
    acc_ref[...] = dot(act, down_ref[shard(size, peer(0)), :])


def down_rest_body(n_tp, acc_ref, down_ref, *refs):
    recv_refs, out_ref, wide = refs[:-2], refs[-2], refs[-1]
    slots, width = acc_ref.shape
    split = width // LANES
    chunks = len(recv_refs) // (n_tp - 1)
    size = recv_refs[0].shape[1] * chunks
    acts = []
    for step in range(1, n_tp):
        parts = recv_refs[(step - 1) * chunks : step * chunks]
        acts.append(jnp.concatenate([ref[...] for ref in parts], axis=1))
    for q in range(0, split, 2):
        cols = slice(q * LANES, (q + 2) * LANES)
        rows = acc_ref[:, cols]
        for step, act in enumerate(acts, 1):
            rows = rows + dot(act, down_ref[shard(size, peer(n_tp - step)), cols])
        wide[pl.ds(q, slots, stride=split), :] = rows[:, :LANES]
        wide[pl.ds(q + 1, slots, stride=split), :] = rows[:, LANES:]
    out_ref[...] = wide[...].astype(BF16)


def combine_body(back_ref, comb_ref, shared_ref, out_ref, wide):
    _, width = out_ref.shape
    slots = comb_ref.shape[1]
    split = width // LANES
    wide[...] = back_ref[...].astype(F32)
    comb = comb_ref[...]
    high = comb.astype(BF16)
    rest = comb - high.astype(F32)
    mid = rest.astype(BF16)
    for q in range(0, split, 2):
        cols = slice(q * LANES, (q + 2) * LANES)
        values = jnp.concatenate(
            [
                wide[pl.ds(q, slots, stride=split), :].astype(BF16),
                wide[pl.ds(q + 1, slots, stride=split), :].astype(BF16),
            ],
            axis=1,
        )
        total = shared_ref[:, cols] + dot(mid, values) + dot(high, values)
        out_ref[:, cols] = total.astype(BF16)


def shift(value, step):
    size = lax.axis_size("tp")
    return lax.ppermute(value, "tp", [(i, (i + step) % size) for i in range(size)])


def experts_plain(arrived, gain, gate_w, up_w, down_w, slots, width):
    values = arrived.reshape(slots, width).astype(F32)
    total = lax.psum(jnp.sum(values * values, axis=1, keepdims=True), "tp")
    normed = values * lax.rsqrt(total / (width * lax.axis_size("tp")) + 1e-06) * gain
    rows = normed.astype(BF16)
    gate, up = (
        lax.psum_scatter(dot(rows, w), "tp", scatter_dimension=1, tiled=True)
        for w in (gate_w, up_w)
    )
    act = lax.all_gather((jax.nn.silu(gate) * up).astype(BF16), "tp", axis=1, tiled=True)
    return dot(act, down_w).astype(BF16).reshape(arrived.shape)


def local(
    tokens,
    norm_gain,
    routes,
    route_weights,
    expert_gate,
    expert_up,
    expert_down,
    shared_gate,
    shared_up,
    shared_down,
):
    tok, width = tokens.shape
    picks = routes.shape[1]
    n_tp, n_ep = lax.axis_size("tp"), lax.axis_size("ep")
    cap = max(2, tok * picks // n_ep + 1)
    slots = n_ep * cap
    split = width // LANES
    hidden = expert_gate.shape[2]
    size = hidden // n_tp
    tok_rows = -(-tok // 16) * 16
    cols = 2 * hidden + LANES
    sds = jax.ShapeDtypeStruct
    sem = pltpu.SemaphoreType.DMA
    wide = pltpu.VMEM((slots * split, LANES), F32)
    block = sds((slots * split, LANES), BF16)
    gain = norm_gain.reshape(1, width)
    gate_w, up_w, down_w = expert_gate[0], expert_up[0], expert_down[0]
    work = 4 * slots * width * size

    def exchange(value):
        blocks = value.reshape(n_ep, cap * split, LANES)
        moved = lax.all_to_all(blocks, "ep", split_axis=0, concat_axis=0, tiled=True)
        return moved.reshape(slots * split, LANES)

    def after(value, *others):
        return lax.optimization_barrier((value,) + others)

    def shared_in(tokens, gain):
        keep, send = call(
            shared_in_body,
            (sds((tok_rows, cols), F32), sds((tok_rows, cols), BF16)),
            [VMEM] * 4,
            (),
            4 * 128 * width * hidden,
        )(tokens, gain, shared_gate, shared_up)
        return keep, [shift(send, step) for step in range(1, n_tp)]

    def shared_out(keep, received):
        return call(
            functools.partial(shared_out_body, width * n_tp),
            sds((tok, width), F32),
            [VMEM] * (n_tp + 1),
            (),
            2 * 128 * width * hidden,
        )(keep, *received, shared_down)

    outgoing, comb = call(
        functools.partial(dispatch_body, cap),
        (block, sds((tok, slots), F32)),
        [HBM] * 3,
        [
            wide,
            pltpu.VMEM((tok, width), BF16),
            pltpu.VMEM((picks, tok), jnp.int32),
            pltpu.VMEM((picks, tok), F32),
            sem((3,)),
        ],
        AHEAD,
    )(*map(stored, (tokens, routes.T, route_weights.T)))
    arrived = exchange(outgoing)
    if size % LANES != 0:
        arrived, tokens, gain = after(arrived, tokens, gain)
        shared_keep, shared_received = shared_in(tokens, gain)
        result = experts_plain(arrived, gain, gate_w, up_w, down_w, slots, width)
    else:
        chunks = 2 if size % (2 * LANES) == 0 else 1
        part = size // chunks
        n_send = n_tp - 1

        def sends(extra):
            return tuple(sds((slots, 2 * part + extra), BF16) for _ in range(n_send))

        def shifted(values):
            return [shift(value, step) for step, value in enumerate(values, 1)]

        *sent, lhs, tail = call(
            functools.partial(expert_first_body, n_send, chunks),
            sends(LANES) + (sds((slots, width), BF16), sds((slots, LANES), F32)),
            [VMEM] * (4 + N_HELD),
            [wide],
            work * n_send // chunks,
        )(arrived, gain, gate_w, up_w, shared_gate, shared_up, down_w, shared_down)
        received = [shifted(sent)]
        for chunk in range(1, chunks):
            sent = call(
                functools.partial(expert_later_body, chunk, chunks),
                sends(0),
                [VMEM] * 3,
                (),
                work * n_send // chunks,
            )(lhs, gate_w, up_w)
            lhs, *sent = after(lhs, *sent)
            received.append(shifted(sent))
        keeps = call(
            expert_keep_body,
            (sds((slots, 2 * part), F32),) * chunks,
            [VMEM] * 3,
            (),
            work,
        )(lhs, gate_w, up_w)
        lhs, tokens, gain = after(lhs, tokens, gain)
        shared_keep, shared_received = shared_in(tokens, gain)
        act, scale = call(
            functools.partial(first_mid_body, width * n_tp),
            (sds((slots, part), BF16), sds((slots, LANES), F32)),
            [VMEM] * (n_tp + 1),
            (),
            10 * slots * part,
        )(keeps[0], tail, *received[0])
        own = [act]
        acts = [[shift(act, step)] for step in range(1, n_tp)]
        for chunk in range(1, chunks):
            act = call(
                later_mid_body,
                sds((slots, part), BF16),
                [VMEM] * (n_tp + 1),
                (),
                10 * slots * part,
            )(keeps[chunk], scale, *received[chunk])
            own.append(act)
            for step in range(1, n_tp):
                acts[step - 1].append(shift(act, step))
        acc = call(
            down_keep_body,
            sds((slots, width), F32),
            [VMEM] * (chunks + 1),
            (),
            work // 2,
        )(down_w, *own)
        result = call(
            functools.partial(down_rest_body, n_tp),
            block,
            [VMEM] * (2 + chunks * n_send),
            [wide],
            work // 2 * n_send,
        )(acc, down_w, *(act for parts in acts for act in parts))
    shared = shared_out(shared_keep, shared_received)
    result, shared = after(result, shared)
    back = exchange(result)
    return call(
        combine_body, sds((tok, width), BF16), [VMEM] * 3, [wide], AHEAD // 10**4
    )(back, comb, shared)


def solution(mesh):
    placed = (
        P("ep", "tp"),
        P("tp"),
        P("ep", None),
        P("ep", None),
        P("ep", "tp", None),
        P("ep", "tp", None),
        P("ep", None, "tp"),
        P("tp", None),
        P("tp", None),
        P(None, "tp"),
    )

    return jax.shard_map(
        local, mesh=mesh, in_specs=placed, out_specs=P("ep", "tp"), check_vma=False
    )
```

profile of v0, /device:TPU:0, one launch (start us, length us, event | category | flops | bytes accessed | tf_op | source)
XLA Modules:
  0.0 50.3 jit_solution(5106851242364508398)
XLA Ops:
  0.0 0.0 copy-start
  0.0 0.0 copy-start.1
  0.0 0.0 copy-start.2
  0.0 0.0 copy-start.3
  0.0 0.0 copy-start.4
  0.0 0.0 copy-start.5
  0.0 0.0 copy-start.7
  0.0 1.4 %shard_map.100 = (bf16[1280,128]{1,0:T(8,128)(2,1)S(1)}, f32[12,80]{1,0:T(8,128)S(1)}) custom-call(bf16[12,2048]{1,0:T(8,128)(2,1)} %tok_ref, s32[6,12]{1,0:T(8,128)} %bitcast.25, f32[6,12]{1,0:T(8,128)} %bitcast.26), custom_call_target="tpu_custom_call" | custom-call | flops 999999995904 | tf_op jit(solution)/shard_map/pallas_call | solution.py:318
  1.4 18.5 %all_to_all.10 = bf16[16,80,128]{2,1,0:T(8,128)(2,1)S(1)} all-to-all(bf16[16,80,128]{2,1,0:T(8,128)(2,1)S(1)} %bitcast.22), channel_id=1, replica_groups=mesh['ep'=16,'tp'=2] {'ep'}, dimensions={0} | all-to-all | bytes 655360 | tf_op jit(solution)/shard_map/all_to_all | solution.py:293
  20.0 0.0 copy-done
  20.0 0.0 copy-done.1
  20.0 0.0 copy-done.2
  20.0 0.0 copy-done.3
  20.0 0.0 copy-done.4
  20.0 0.0 copy-done.5
  20.0 0.0 copy-done.7
  20.0 0.8 %shard_map.101 = (bf16[80,640]{1,0:T(8,128)(2,1)S(1)}, bf16[80,2048]{1,0:T(8,128)(2,1)S(1)}, f32[80,128]{1,0:T(8,128)S(1)}) custom-call(bf16[1280,128]{1,0:T(8,128)(2,1)S(1)} %bitcast.21, f32[1,2048]{1,0:T(1,128)S(1)} %bitcast.23, bf16[2048,1024]{1,0:T(8,128)(2,1)S(1)} %bitcast.10, bf16[2048,1024]{1,0:T(8,128)(2,1)S(1)} %bitcast.13, ...), custom_call_target="tpu_custom_call" | custom-call | flops 167772160 | tf_op jit(solution)/shard_map/pallas_call | solution.py:347
  20.8 0.0 copy-start.6
  20.8 0.5 %shard_map.102 = bf16[80,512]{1,0:T(8,128)(2,1)S(1)} custom-call(bf16[80,2048]{1,0:T(8,128)(2,1)S(1)} %get-tuple-element.24.lhs_ref, bf16[2048,1024]{1,0:T(8,128)(2,1)S(1)} %bitcast.11, bf16[2048,1024]{1,0:T(8,128)(2,1)S(1)} %bitcast.14), custom_call_target="tpu_custom_call" | custom-call | flops 167772160 | tf_op jit(solution)/shard_map/pallas_call | solution.py:356
  21.3 1.6 %collective-permute-start.1 = (bf16[80,512]{1,0:T(8,128)(2,1)S(1)}, bf16[80,512]{1,0:T(8,128)(2,1)S(1)}, u32[]{:S(2)}, u32[]{:S(2)}) collective-permute-start(bf16[80,512]{1,0:T(8,128)(2,1)S(1)} %shard_map.102), channel_id=1, source_target_pairs={{0,1},{1,0},{2,3},{3,2},{4,5},{5,4},{6,7},{7,6},{8,9},{9,8},{10,11... | collective-permute-start | bytes 245768 | tf_op jit(solution)/shard_map/ppermute | solution.py:245
  22.9 0.5 %collective-permute-start = (bf16[80,640]{1,0:T(8,128)(2,1)S(1)}, bf16[80,640]{1,0:T(8,128)(2,1)S(1)}, u32[]{:S(2)}, u32[]{:S(2)}) collective-permute-start(bf16[80,640]{1,0:T(8,128)(2,1)S(1)} %get-tuple-element.27), channel_id=1, source_target_pairs={{0,1},{1,0},{2,3},{3,2},{4,5},{5,4},{6,7},{7,6},{8,9},{9,8},{10,11... | collective-permute-start | bytes 307208 | tf_op jit(solution)/shard_map/ppermute | solution.py:245
  23.4 0.0 copy-done.6
  23.4 1.2 %shard_map.108 = (f32[16,2176]{1,0:T(8,128)S(1)}, bf16[16,2176]{1,0:T(8,128)(2,1)S(1)}) custom-call(bf16[12,2048]{1,0:T(8,128)(2,1)S(1)} %copy-done.6, f32[1,2048]{1,0:T(1,128)S(1)} %bitcast.24, bf16[2048,1024]{1,0:T(8,128)(2,1)S(1)} %copy-done.3, bf16[2048,1024]{1,0:T(8,128)(2,1)S(1)} %copy-done.4), custom_call_target="tpu_custom_call" | custom-call | flops 1073741824 | tf_op jit(solution)/shard_map/pallas_call | solution.py:300
  24.6 1.5 %collective-permute-start.4 = (bf16[16,2176]{1,0:T(8,128)(2,1)S(1)}, bf16[16,2176]{1,0:T(8,128)(2,1)S(1)}, u32[]{:S(2)}, u32[]{:S(2)}) collective-permute-start(bf16[16,2176]{1,0:T(8,128)(2,1)S(1)} %get-tuple-element.35), channel_id=1, source_target_pairs={{0,1},{1,0},{2,3},{3,2},{4,5},{5,4},{6,7},{7,6},{8,9},{9,8},{10,11... | collective-permute-start | bytes 208904 | tf_op jit(solution)/shard_map/ppermute | solution.py:245
  26.2 0.9 %shard_map.103 = (f32[80,512]{1,0:T(8,128)S(1)}, f32[80,512]{1,0:T(8,128)S(1)}) custom-call(bf16[80,2048]{1,0:T(8,128)(2,1)S(1)} %get-tuple-element.24.lhs_ref, bf16[2048,1024]{1,0:T(8,128)(2,1)S(1)} %bitcast.12, bf16[2048,1024]{1,0:T(8,128)(2,1)S(1)} %bitcast.15), custom_call_target="tpu_custom_call" | custom-call | flops 335544320 | tf_op jit(solution)/shard_map/pallas_call | solution.py:365
  27.0 1.6 %collective-permute-done.refs_0_ = bf16[80,640]{1,0:T(8,128)(2,1)S(1)} collective-permute-done((bf16[80,640]{1,0:T(8,128)(2,1)S(1)}, bf16[80,640]{1,0:T(8,128)(2,1)S(1)}, u32[]{:S(2)}, u32[]{:S(2)}) %collective-permute-start) | collective-permute-done | bytes 102432 | tf_op jit(solution)/shard_map/ppermute | solution.py:245
  28.7 0.1 shard_map.104
  28.8 0.0 collective-permute-done.1.refs_0_
  28.8 0.1 shard_map.105.refs_1_
  28.9 1.7 %collective-permute-start.3 = (bf16[80,256]{1,0:T(8,128)(2,1)S(1)}, bf16[80,256]{1,0:T(8,128)(2,1)S(1)}, u32[]{:S(2)}, u32[]{:S(2)}) collective-permute-start(bf16[80,256]{1,0:T(8,128)(2,1)S(1)} %shard_map.105.refs_1_), channel_id=1, source_target_pairs={{0,1},{1,0},{2,3},{3,2},{4,5},{5,4},{6,7},{7,6},{8,9},{9,8},{10,11... | collective-permute-start | bytes 122888 | tf_op jit(solution)/shard_map/ppermute | solution.py:245
  30.6 0.4 collective-permute-start.2
  31.0 0.0 collective-permute-done.4.refs_0_
  31.0 0.7 %shard_map.109.shared_ref = f32[12,2048]{1,0:T(8,128)S(1)} custom-call(f32[16,2176]{1,0:T(8,128)S(1)} %get-tuple-element.34.keep_ref, bf16[16,2176]{1,0:T(8,128)(2,1)S(1)} %collective-permute-done.4.refs_0_, bf16[1024,2048]{1,0:T(8,128)(2,1)S(1)} %copy-done.5), custom_call_target="tpu_custom_call" | custom-call | flops 536870912 | tf_op jit(solution)/shard_map/pallas_call | solution.py:310
  31.7 0.5 shard_map.106.acc_ref
  32.2 0.7 %collective-permute-done.3.refs_1_ = bf16[80,256]{1,0:T(8,128)(2,1)S(1)} collective-permute-done((bf16[80,256]{1,0:T(8,128)(2,1)S(1)}, bf16[80,256]{1,0:T(8,128)(2,1)S(1)}, u32[]{:S(2)}, u32[]{:S(2)}) %collective-permute-start.3) | collective-permute-done | bytes 40992 | tf_op jit(solution)/shard_map/ppermute | solution.py:245
  33.0 1.6 %collective-permute-done.2.refs_0_ = bf16[80,256]{1,0:T(8,128)(2,1)S(1)} collective-permute-done((bf16[80,256]{1,0:T(8,128)(2,1)S(1)}, bf16[80,256]{1,0:T(8,128)(2,1)S(1)}, u32[]{:S(2)}, u32[]{:S(2)}) %collective-permute-start.2) | collective-permute-done | bytes 40992 | tf_op jit(solution)/shard_map/ppermute | solution.py:245
  34.6 0.6 %shard_map.107 = bf16[1280,128]{1,0:T(8,128)(2,1)S(1)} custom-call(f32[80,2048]{1,0:T(8,128)S(1)} %shard_map.106.acc_ref, bf16[1024,2048]{1,0:T(8,128)(2,1)S(1)} %bitcast.18, bf16[80,256]{1,0:T(8,128)(2,1)S(1)} %collective-permute-done.2.refs_0_, bf16[80,256]{1,0:T(8,128)(2,1)S(1)} %collective-permute-done.3.refs_1_), custom_call_target="tpu_custom_call" | custom-call | flops 167772160 | tf_op jit(solution)/shard_map/pallas_call | solution.py:401
  35.2 14.1 %all_to_all.11 = bf16[16,80,128]{2,1,0:T(8,128)(2,1)S(1)} all-to-all(bf16[16,80,128]{2,1,0:T(8,128)(2,1)S(1)} %bitcast.19), channel_id=1, replica_groups=mesh['ep'=16,'tp'=2] {'ep'}, dimensions={0} | all-to-all | bytes 655360 | tf_op jit(solution)/shard_map/all_to_all | solution.py:293
  49.3 1.0 %shard_map.110 = bf16[12,2048]{1,0:T(8,128)(2,1)} custom-call(bf16[1280,128]{1,0:T(8,128)(2,1)S(1)} %bitcast.20, f32[12,80]{1,0:T(8,128)S(1)} %get-tuple-element.37.comb_ref, f32[12,2048]{1,0:T(8,128)S(1)} %shard_map.109.shared_ref), custom_call_target="tpu_custom_call" | custom-call | flops 100000000 | tf_op jit(solution)/shard_map/pallas_call | solution.py:411
Async XLA Ops:
  0.0 20.0 %copy-start = (bf16[1,2048,1024]{2,1,0:T(8,128)(2,1)S(1)}, bf16[1,2048,1024]{2,1,0:T(8,128)(2,1)}, u32[]{:S(2)}) copy-start(bf16[1,2048,1024]{2,1,0:T(8,128)(2,1)} %param.14) | copy-start | bytes 12582916
  0.0 20.0 %copy-start.1 = (bf16[1,2048,1024]{2,1,0:T(8,128)(2,1)S(1)}, bf16[1,2048,1024]{2,1,0:T(8,128)(2,1)}, u32[]{:S(2)}) copy-start(bf16[1,2048,1024]{2,1,0:T(8,128)(2,1)} %param.15) | copy-start | bytes 12582916
  0.0 20.0 %copy-start.2 = (bf16[1,1024,2048]{2,1,0:T(8,128)(2,1)S(1)}, bf16[1,1024,2048]{2,1,0:T(8,128)(2,1)}, u32[]{:S(2)}) copy-start(bf16[1,1024,2048]{2,1,0:T(8,128)(2,1)} %param.16) | copy-start | bytes 12582916
  0.0 20.0 %copy-start.3 = (bf16[2048,1024]{1,0:T(8,128)(2,1)S(1)}, bf16[2048,1024]{1,0:T(8,128)(2,1)}, u32[]{:S(2)}) copy-start(bf16[2048,1024]{1,0:T(8,128)(2,1)} %gate_ref.1) | copy-start | bytes 12582916
  0.0 20.0 %copy-start.4 = (bf16[2048,1024]{1,0:T(8,128)(2,1)S(1)}, bf16[2048,1024]{1,0:T(8,128)(2,1)}, u32[]{:S(2)}) copy-start(bf16[2048,1024]{1,0:T(8,128)(2,1)} %up_ref.1) | copy-start | bytes 12582916
  0.0 20.0 %copy-start.5 = (bf16[1024,2048]{1,0:T(8,128)(2,1)S(1)}, bf16[1024,2048]{1,0:T(8,128)(2,1)}, u32[]{:S(2)}) copy-start(bf16[1024,2048]{1,0:T(8,128)(2,1)} %refs_1_.3) | copy-start | bytes 12582916
  0.0 20.0 %copy-start.7 = (f32[2048]{0:T(1024)S(1)}, f32[2048]{0:T(1024)}, u32[]{:S(2)}) copy-start(f32[2048]{0:T(1024)} %param.11) | copy-start | bytes 24580
  20.8 2.6 %copy-start.6 = (bf16[12,2048]{1,0:T(8,128)(2,1)S(1)}, bf16[12,2048]{1,0:T(8,128)(2,1)}, u32[]{:S(2)}) copy-start(bf16[12,2048]{1,0:T(8,128)(2,1)} %tok_ref) | copy-start | bytes 147460
  21.3 7.5 %collective-permute-start.1 = (bf16[80,512]{1,0:T(8,128)(2,1)S(1)}, bf16[80,512]{1,0:T(8,128)(2,1)S(1)}, u32[]{:S(2)}, u32[]{:S(2)}) collective-permute-start(bf16[80,512]{1,0:T(8,128)(2,1)S(1)} %shard_map.102), channel_id=1, source_target_pairs={{0,1},{1,0},{2,3},{3,2},{4,5},{5,4},{6,7},{7,6},{8,9},{9,8},{10,11... | collective-permute-start | bytes 245768 | tf_op jit(solution)/shard_map/ppermute | solution.py:245
  22.9 5.8 %collective-permute-start = (bf16[80,640]{1,0:T(8,128)(2,1)S(1)}, bf16[80,640]{1,0:T(8,128)(2,1)S(1)}, u32[]{:S(2)}, u32[]{:S(2)}) collective-permute-start(bf16[80,640]{1,0:T(8,128)(2,1)S(1)} %get-tuple-element.27), channel_id=1, source_target_pairs={{0,1},{1,0},{2,3},{3,2},{4,5},{5,4},{6,7},{7,6},{8,9},{9,8},{10,11... | collective-permute-start | bytes 307208 | tf_op jit(solution)/shard_map/ppermute | solution.py:245
  24.6 6.4 %collective-permute-start.4 = (bf16[16,2176]{1,0:T(8,128)(2,1)S(1)}, bf16[16,2176]{1,0:T(8,128)(2,1)S(1)}, u32[]{:S(2)}, u32[]{:S(2)}) collective-permute-start(bf16[16,2176]{1,0:T(8,128)(2,1)S(1)} %get-tuple-element.35), channel_id=1, source_target_pairs={{0,1},{1,0},{2,3},{3,2},{4,5},{5,4},{6,7},{7,6},{8,9},{9,8},{10,11... | collective-permute-start | bytes 208904 | tf_op jit(solution)/shard_map/ppermute | solution.py:245
  28.9 4.1 %collective-permute-start.3 = (bf16[80,256]{1,0:T(8,128)(2,1)S(1)}, bf16[80,256]{1,0:T(8,128)(2,1)S(1)}, u32[]{:S(2)}, u32[]{:S(2)}) collective-permute-start(bf16[80,256]{1,0:T(8,128)(2,1)S(1)} %shard_map.105.refs_1_), channel_id=1, source_target_pairs={{0,1},{1,0},{2,3},{3,2},{4,5},{5,4},{6,7},{7,6},{8,9},{9,8},{10,11... | collective-permute-start | bytes 122888 | tf_op jit(solution)/shard_map/ppermute | solution.py:245
  30.6 4.0 %collective-permute-start.2 = (bf16[80,256]{1,0:T(8,128)(2,1)S(1)}, bf16[80,256]{1,0:T(8,128)(2,1)S(1)}, u32[]{:S(2)}, u32[]{:S(2)}) collective-permute-start(bf16[80,256]{1,0:T(8,128)(2,1)S(1)} %get-tuple-element.28.refs_0_), channel_id=1, source_target_pairs={{0,1},{1,0},{2,3},{3,2},{4,5},{5,4},{6,7},{7,6},{8,9},{9,8},{10,11... | collective-permute-start | bytes 122888 | tf_op jit(solution)/shard_map/ppermute | solution.py:245
where the time goes:
time: 50.5 us; the launch traced here: 50.3 us
  blocking collectives  32.7 us (65%)
  Pallas kernels  7.8 us (15%)
  starting transfers between devices  5.72 us (11%)
  waiting for transfers between devices  4.02 us (8%)
    all_to_all x2, blocking collectives, exchange(): lax.all_to_all(blocks, 'ep', split_axis=0, concat_axis=0, tiled=True)  32.7 us
    ppermute x5, starting transfers between devices, shift(): lax.ppermute(value, 'tp', [(i, (i + step) % size) for i in range(size)])  5.72 us
    ppermute x5, waiting for transfers between devices, shift(): lax.ppermute(value, 'tp', [(i, (i + step) % size) for i in range(size)])  4.02 us
    pallas_call x1, Pallas kernels, local(): call(functools.partial(dispatch_body, cap), (block, sds((tok, slots), F32...  1.38 us
    pallas_call x1, Pallas kernels, shared_in(): call(shared_in_body, (sds((tok_rows, cols), F32), sds((tok_rows, cols), B...  1.2 us
  transfers between devices with their start and end apart: 5, of which 3 were waited for; matrix products, arithmetic and copies ran while one was open for 0% of the time, Pallas kernels for 7%

commit v1 on v0

--- a/solution.py
+++ b/solution.py
@@ -93,7 +93,7 @@
 
 def squares_tail(total):
     lane = lax.broadcasted_iota(jnp.int32, (total.shape[0], LANES), 1)
-    high = total.astype(BF16).astype(F32)
+    high = jnp.minimum(total, 3.3e38).astype(BF16).astype(F32)
     return jnp.where(lane == 0, high, jnp.where(lane == 1, total - high, 0.0))
 
 
@@ -114,8 +114,9 @@
 
 
 def hidden_units(total, scale, hidden):
-    gate = total[:, :hidden] * scale
-    up = total[:, hidden : 2 * hidden] * scale
+    alive = scale > 0.0
+    gate = jnp.where(alive, total[:, :hidden] * scale, 0.0)
+    up = jnp.where(alive, total[:, hidden : 2 * hidden] * scale, 0.0)
     return (gate / (1.0 + jnp.exp(-gate)) * up).astype(BF16)
 
 

time: 50.5 us -> 50.6 us (level)
  no operation moved by 1% of the time
where the time goes in v1:
time: 50.6 us; the launch traced here: 50.4 us
  blocking collectives  32.6 us (64%)
  Pallas kernels  7.83 us (15%)
  starting transfers between devices  5.71 us (11%)
  waiting for transfers between devices  4.02 us (8%)
    all_to_all x2, blocking collectives, exchange(): lax.all_to_all(blocks, 'ep', split_axis=0, concat_axis=0, tiled=True)  32.6 us
    ppermute x5, starting transfers between devices, shift(): lax.ppermute(value, 'tp', [(i, (i + step) % size) for i in range(size)])  5.71 us
    ppermute x5, waiting for transfers between devices, shift(): lax.ppermute(value, 'tp', [(i, (i + step) % size) for i in range(size)])  4.02 us
    pallas_call x1, Pallas kernels, local(): call(functools.partial(dispatch_body, cap), (block, sds((tok, slots), F32...  1.38 us
    pallas_call x1, Pallas kernels, shared_in(): call(shared_in_body, (sds((tok_rows, cols), F32), sds((tok_rows, cols), B...  1.21 us
  transfers between devices with their start and end apart: 5, of which 3 were waited for; matrix products, arithmetic and copies ran while one was open for 0% of the time, Pallas kernels for 7%

profile of v1, /device:TPU:0, one launch (start us, length us, event | category | flops | bytes accessed | tf_op | source)
XLA Modules:
  0.0 50.4 jit_solution(13413501458702178735)
XLA Ops:
  0.0 0.0 copy-start
  0.0 0.0 copy-start.1
  0.0 0.0 copy-start.2
  0.0 0.0 copy-start.3
  0.0 0.0 copy-start.4
  0.0 0.0 copy-start.5
  0.0 0.0 copy-start.7
  0.0 1.4 %shard_map.100 = (bf16[1280,128]{1,0:T(8,128)(2,1)S(1)}, f32[12,80]{1,0:T(8,128)S(1)}) custom-call(bf16[12,2048]{1,0:T(8,128)(2,1)} %tok_ref, s32[6,12]{1,0:T(8,128)} %bitcast.25, f32[6,12]{1,0:T(8,128)} %bitcast.26), custom_call_target="tpu_custom_call" | custom-call | flops 999999995904 | tf_op jit(solution)/shard_map/pallas_call | solution.py:319
  1.4 18.5 %all_to_all.10 = bf16[16,80,128]{2,1,0:T(8,128)(2,1)S(1)} all-to-all(bf16[16,80,128]{2,1,0:T(8,128)(2,1)S(1)} %bitcast.22), channel_id=1, replica_groups=mesh['ep'=16,'tp'=2] {'ep'}, dimensions={0} | all-to-all | bytes 655360 | tf_op jit(solution)/shard_map/all_to_all | solution.py:294
  20.0 0.0 copy-done
  20.0 0.0 copy-done.1
  20.0 0.0 copy-done.2
  20.0 0.0 copy-done.3
  20.0 0.0 copy-done.4
  20.0 0.0 copy-done.5
  20.0 0.0 copy-done.7
  20.0 0.8 %shard_map.101 = (bf16[80,640]{1,0:T(8,128)(2,1)S(1)}, bf16[80,2048]{1,0:T(8,128)(2,1)S(1)}, f32[80,128]{1,0:T(8,128)S(1)}) custom-call(bf16[1280,128]{1,0:T(8,128)(2,1)S(1)} %bitcast.21, f32[1,2048]{1,0:T(1,128)S(1)} %bitcast.23, bf16[2048,1024]{1,0:T(8,128)(2,1)S(1)} %bitcast.10, bf16[2048,1024]{1,0:T(8,128)(2,1)S(1)} %bitcast.13, ...), custom_call_target="tpu_custom_call" | custom-call | flops 167772160 | tf_op jit(solution)/shard_map/pallas_call | solution.py:348
  20.8 0.0 copy-start.6
  20.8 0.5 %shard_map.102 = bf16[80,512]{1,0:T(8,128)(2,1)S(1)} custom-call(bf16[80,2048]{1,0:T(8,128)(2,1)S(1)} %get-tuple-element.24.lhs_ref, bf16[2048,1024]{1,0:T(8,128)(2,1)S(1)} %bitcast.11, bf16[2048,1024]{1,0:T(8,128)(2,1)S(1)} %bitcast.14), custom_call_target="tpu_custom_call" | custom-call | flops 167772160 | tf_op jit(solution)/shard_map/pallas_call | solution.py:357
  21.3 1.6 %collective-permute-start.1 = (bf16[80,512]{1,0:T(8,128)(2,1)S(1)}, bf16[80,512]{1,0:T(8,128)(2,1)S(1)}, u32[]{:S(2)}, u32[]{:S(2)}) collective-permute-start(bf16[80,512]{1,0:T(8,128)(2,1)S(1)} %shard_map.102), channel_id=1, source_target_pairs={{0,1},{1,0},{2,3},{3,2},{4,5},{5,4},{6,7},{7,6},{8,9},{9,8},{10,11... | collective-permute-start | bytes 245768 | tf_op jit(solution)/shard_map/ppermute | solution.py:246
  22.9 0.5 %collective-permute-start = (bf16[80,640]{1,0:T(8,128)(2,1)S(1)}, bf16[80,640]{1,0:T(8,128)(2,1)S(1)}, u32[]{:S(2)}, u32[]{:S(2)}) collective-permute-start(bf16[80,640]{1,0:T(8,128)(2,1)S(1)} %get-tuple-element.27), channel_id=1, source_target_pairs={{0,1},{1,0},{2,3},{3,2},{4,5},{5,4},{6,7},{7,6},{8,9},{9,8},{10,11... | collective-permute-start | bytes 307208 | tf_op jit(solution)/shard_map/ppermute | solution.py:246
  23.4 0.0 copy-done.6
  23.4 1.2 %shard_map.108 = (f32[16,2176]{1,0:T(8,128)S(1)}, bf16[16,2176]{1,0:T(8,128)(2,1)S(1)}) custom-call(bf16[12,2048]{1,0:T(8,128)(2,1)S(1)} %copy-done.6, f32[1,2048]{1,0:T(1,128)S(1)} %bitcast.24, bf16[2048,1024]{1,0:T(8,128)(2,1)S(1)} %copy-done.3, bf16[2048,1024]{1,0:T(8,128)(2,1)S(1)} %copy-done.4), custom_call_target="tpu_custom_call" | custom-call | flops 1073741824 | tf_op jit(solution)/shard_map/pallas_call | solution.py:301
  24.6 1.5 %collective-permute-start.4 = (bf16[16,2176]{1,0:T(8,128)(2,1)S(1)}, bf16[16,2176]{1,0:T(8,128)(2,1)S(1)}, u32[]{:S(2)}, u32[]{:S(2)}) collective-permute-start(bf16[16,2176]{1,0:T(8,128)(2,1)S(1)} %get-tuple-element.35), channel_id=1, source_target_pairs={{0,1},{1,0},{2,3},{3,2},{4,5},{5,4},{6,7},{7,6},{8,9},{9,8},{10,11... | collective-permute-start | bytes 208904 | tf_op jit(solution)/shard_map/ppermute | solution.py:246
  26.2 0.9 %shard_map.103 = (f32[80,512]{1,0:T(8,128)S(1)}, f32[80,512]{1,0:T(8,128)S(1)}) custom-call(bf16[80,2048]{1,0:T(8,128)(2,1)S(1)} %get-tuple-element.24.lhs_ref, bf16[2048,1024]{1,0:T(8,128)(2,1)S(1)} %bitcast.12, bf16[2048,1024]{1,0:T(8,128)(2,1)S(1)} %bitcast.15), custom_call_target="tpu_custom_call" | custom-call | flops 335544320 | tf_op jit(solution)/shard_map/pallas_call | solution.py:366
  27.0 1.6 %collective-permute-done.refs_0_ = bf16[80,640]{1,0:T(8,128)(2,1)S(1)} collective-permute-done((bf16[80,640]{1,0:T(8,128)(2,1)S(1)}, bf16[80,640]{1,0:T(8,128)(2,1)S(1)}, u32[]{:S(2)}, u32[]{:S(2)}) %collective-permute-start) | collective-permute-done | bytes 102432 | tf_op jit(solution)/shard_map/ppermute | solution.py:246
  28.7 0.1 shard_map.104
  28.8 0.0 collective-permute-done.1.refs_0_
  28.8 0.1 shard_map.105.refs_1_
  28.9 1.7 %collective-permute-start.3 = (bf16[80,256]{1,0:T(8,128)(2,1)S(1)}, bf16[80,256]{1,0:T(8,128)(2,1)S(1)}, u32[]{:S(2)}, u32[]{:S(2)}) collective-permute-start(bf16[80,256]{1,0:T(8,128)(2,1)S(1)} %shard_map.105.refs_1_), channel_id=1, source_target_pairs={{0,1},{1,0},{2,3},{3,2},{4,5},{5,4},{6,7},{7,6},{8,9},{9,8},{10,11... | collective-permute-start | bytes 122888 | tf_op jit(solution)/shard_map/ppermute | solution.py:246
  30.6 0.4 collective-permute-start.2
  31.0 0.0 collective-permute-done.4.refs_0_
  31.0 0.7 %shard_map.109.shared_ref = f32[12,2048]{1,0:T(8,128)S(1)} custom-call(f32[16,2176]{1,0:T(8,128)S(1)} %get-tuple-element.34.keep_ref, bf16[16,2176]{1,0:T(8,128)(2,1)S(1)} %collective-permute-done.4.refs_0_, bf16[1024,2048]{1,0:T(8,128)(2,1)S(1)} %copy-done.5), custom_call_target="tpu_custom_call" | custom-call | flops 536870912 | tf_op jit(solution)/shard_map/pallas_call | solution.py:311
  31.8 0.5 shard_map.106.acc_ref
  32.3 0.7 %collective-permute-done.3.refs_1_ = bf16[80,256]{1,0:T(8,128)(2,1)S(1)} collective-permute-done((bf16[80,256]{1,0:T(8,128)(2,1)S(1)}, bf16[80,256]{1,0:T(8,128)(2,1)S(1)}, u32[]{:S(2)}, u32[]{:S(2)}) %collective-permute-start.3) | collective-permute-done | bytes 40992 | tf_op jit(solution)/shard_map/ppermute | solution.py:246
  33.0 1.6 %collective-permute-done.2.refs_0_ = bf16[80,256]{1,0:T(8,128)(2,1)S(1)} collective-permute-done((bf16[80,256]{1,0:T(8,128)(2,1)S(1)}, bf16[80,256]{1,0:T(8,128)(2,1)S(1)}, u32[]{:S(2)}, u32[]{:S(2)}) %collective-permute-start.2) | collective-permute-done | bytes 40992 | tf_op jit(solution)/shard_map/ppermute | solution.py:246
  34.6 0.6 %shard_map.107 = bf16[1280,128]{1,0:T(8,128)(2,1)S(1)} custom-call(f32[80,2048]{1,0:T(8,128)S(1)} %shard_map.106.acc_ref, bf16[1024,2048]{1,0:T(8,128)(2,1)S(1)} %bitcast.18, bf16[80,256]{1,0:T(8,128)(2,1)S(1)} %collective-permute-done.2.refs_0_, bf16[80,256]{1,0:T(8,128)(2,1)S(1)} %collective-permute-done.3.refs_1_), custom_call_target="tpu_custom_call" | custom-call | flops 167772160 | tf_op jit(solution)/shard_map/pallas_call | solution.py:402
  35.2 14.1 %all_to_all.11 = bf16[16,80,128]{2,1,0:T(8,128)(2,1)S(1)} all-to-all(bf16[16,80,128]{2,1,0:T(8,128)(2,1)S(1)} %bitcast.19), channel_id=1, replica_groups=mesh['ep'=16,'tp'=2] {'ep'}, dimensions={0} | all-to-all | bytes 655360 | tf_op jit(solution)/shard_map/all_to_all | solution.py:294
  49.4 1.0 %shard_map.110 = bf16[12,2048]{1,0:T(8,128)(2,1)} custom-call(bf16[1280,128]{1,0:T(8,128)(2,1)S(1)} %bitcast.20, f32[12,80]{1,0:T(8,128)S(1)} %get-tuple-element.37.comb_ref, f32[12,2048]{1,0:T(8,128)S(1)} %shard_map.109.shared_ref), custom_call_target="tpu_custom_call" | custom-call | flops 100000000 | tf_op jit(solution)/shard_map/pallas_call | solution.py:412
Async XLA Ops:
  0.0 20.0 %copy-start = (bf16[1,2048,1024]{2,1,0:T(8,128)(2,1)S(1)}, bf16[1,2048,1024]{2,1,0:T(8,128)(2,1)}, u32[]{:S(2)}) copy-start(bf16[1,2048,1024]{2,1,0:T(8,128)(2,1)} %param.14) | copy-start | bytes 12582916
  0.0 20.0 %copy-start.1 = (bf16[1,2048,1024]{2,1,0:T(8,128)(2,1)S(1)}, bf16[1,2048,1024]{2,1,0:T(8,128)(2,1)}, u32[]{:S(2)}) copy-start(bf16[1,2048,1024]{2,1,0:T(8,128)(2,1)} %param.15) | copy-start | bytes 12582916
  0.0 20.0 %copy-start.2 = (bf16[1,1024,2048]{2,1,0:T(8,128)(2,1)S(1)}, bf16[1,1024,2048]{2,1,0:T(8,128)(2,1)}, u32[]{:S(2)}) copy-start(bf16[1,1024,2048]{2,1,0:T(8,128)(2,1)} %param.16) | copy-start | bytes 12582916
  0.0 20.0 %copy-start.3 = (bf16[2048,1024]{1,0:T(8,128)(2,1)S(1)}, bf16[2048,1024]{1,0:T(8,128)(2,1)}, u32[]{:S(2)}) copy-start(bf16[2048,1024]{1,0:T(8,128)(2,1)} %gate_ref.1) | copy-start | bytes 12582916
  0.0 20.0 %copy-start.4 = (bf16[2048,1024]{1,0:T(8,128)(2,1)S(1)}, bf16[2048,1024]{1,0:T(8,128)(2,1)}, u32[]{:S(2)}) copy-start(bf16[2048,1024]{1,0:T(8,128)(2,1)} %up_ref.1) | copy-start | bytes 12582916
  0.0 20.0 %copy-start.5 = (bf16[1024,2048]{1,0:T(8,128)(2,1)S(1)}, bf16[1024,2048]{1,0:T(8,128)(2,1)}, u32[]{:S(2)}) copy-start(bf16[1024,2048]{1,0:T(8,128)(2,1)} %refs_1_.3) | copy-start | bytes 12582916
  0.0 20.0 %copy-start.7 = (f32[2048]{0:T(1024)S(1)}, f32[2048]{0:T(1024)}, u32[]{:S(2)}) copy-start(f32[2048]{0:T(1024)} %param.11) | copy-start | bytes 24580
  20.8 2.6 %copy-start.6 = (bf16[12,2048]{1,0:T(8,128)(2,1)S(1)}, bf16[12,2048]{1,0:T(8,128)(2,1)}, u32[]{:S(2)}) copy-start(bf16[12,2048]{1,0:T(8,128)(2,1)} %tok_ref) | copy-start | bytes 147460
  21.3 7.5 %collective-permute-start.1 = (bf16[80,512]{1,0:T(8,128)(2,1)S(1)}, bf16[80,512]{1,0:T(8,128)(2,1)S(1)}, u32[]{:S(2)}, u32[]{:S(2)}) collective-permute-start(bf16[80,512]{1,0:T(8,128)(2,1)S(1)} %shard_map.102), channel_id=1, source_target_pairs={{0,1},{1,0},{2,3},{3,2},{4,5},{5,4},{6,7},{7,6},{8,9},{9,8},{10,11... | collective-permute-start | bytes 245768 | tf_op jit(solution)/shard_map/ppermute | solution.py:246
  22.9 5.8 %collective-permute-start = (bf16[80,640]{1,0:T(8,128)(2,1)S(1)}, bf16[80,640]{1,0:T(8,128)(2,1)S(1)}, u32[]{:S(2)}, u32[]{:S(2)}) collective-permute-start(bf16[80,640]{1,0:T(8,128)(2,1)S(1)} %get-tuple-element.27), channel_id=1, source_target_pairs={{0,1},{1,0},{2,3},{3,2},{4,5},{5,4},{6,7},{7,6},{8,9},{9,8},{10,11... | collective-permute-start | bytes 307208 | tf_op jit(solution)/shard_map/ppermute | solution.py:246
  24.6 6.4 %collective-permute-start.4 = (bf16[16,2176]{1,0:T(8,128)(2,1)S(1)}, bf16[16,2176]{1,0:T(8,128)(2,1)S(1)}, u32[]{:S(2)}, u32[]{:S(2)}) collective-permute-start(bf16[16,2176]{1,0:T(8,128)(2,1)S(1)} %get-tuple-element.35), channel_id=1, source_target_pairs={{0,1},{1,0},{2,3},{3,2},{4,5},{5,4},{6,7},{7,6},{8,9},{9,8},{10,11... | collective-permute-start | bytes 208904 | tf_op jit(solution)/shard_map/ppermute | solution.py:246
  28.9 4.1 %collective-permute-start.3 = (bf16[80,256]{1,0:T(8,128)(2,1)S(1)}, bf16[80,256]{1,0:T(8,128)(2,1)S(1)}, u32[]{:S(2)}, u32[]{:S(2)}) collective-permute-start(bf16[80,256]{1,0:T(8,128)(2,1)S(1)} %shard_map.105.refs_1_), channel_id=1, source_target_pairs={{0,1},{1,0},{2,3},{3,2},{4,5},{5,4},{6,7},{7,6},{8,9},{9,8},{10,11... | collective-permute-start | bytes 122888 | tf_op jit(solution)/shard_map/ppermute | solution.py:246
  30.6 4.0 %collective-permute-start.2 = (bf16[80,256]{1,0:T(8,128)(2,1)S(1)}, bf16[80,256]{1,0:T(8,128)(2,1)S(1)}, u32[]{:S(2)}, u32[]{:S(2)}) collective-permute-start(bf16[80,256]{1,0:T(8,128)(2,1)S(1)} %get-tuple-element.28.refs_0_), channel_id=1, source_target_pairs={{0,1},{1,0},{2,3},{3,2},{4,5},{5,4},{6,7},{7,6},{8,9},{9,8},{10,11... | collective-permute-start | bytes 122888 | tf_op jit(solution)/shard_map/ppermute | solution.py:246
